TPU v7x, 32 devices: a whole 2x2x4 slice. The times are simulated.
32 devices in a mesh: ep: 8 (over z, y), tp: 4 (over x, core).
Axes of the slice: x: 2, y: 2, z: 4, core: 2. Of those that a mesh axis runs over, the one named last changes fastest.
Arguments:
- resid: bfloat16 [256, 2048], P('ep'), may hold values from -6 to 6
- mix_gain: bfloat16 [2048], replicated, may hold values from 0.099609375 to 1.8984375
- proj_x: bfloat16 [2048, 512], P(None, 'tp'), may hold values from -0.125 to 0.125
- proj_z: bfloat16 [2048, 512], P(None, 'tp'), may hold values from -0.125 to 0.125
- proj_b: bfloat16 [2048, 512], P(None, 'tp'), may hold values from -0.125 to 0.125
- proj_c: bfloat16 [2048, 512], P(None, 'tp'), may hold values from -0.125 to 0.125
- proj_step: bfloat16 [2048, 8], replicated, may hold values from -0.125 to 0.125
- step_bias: float32 [8], P('tp'), may hold values from -5 to -1
- decay_rate: float32 [8], P('tp'), may hold values from 1 to 16
- conv_taps: bfloat16 [3, 4, 512], P(None, None, 'tp'), may hold values from -3 to 3
- conv_state: bfloat16 [256, 3, 3, 512], P('ep', None, None, 'tp'), may hold values from -6 to 6
- scan_state: float32 [256, 8, 64, 128], P('ep', 'tp'), may hold values from -2.5 to 2.5
- inner_gain: bfloat16 [512], P('tp'), may hold values from 0.099609375 to 1.8984375
- proj_out: bfloat16 [512, 2048], P('tp'), may hold values from -0.25 to 0.25
- post_gain: bfloat16 [2048], replicated, may hold values from 0.099609375 to 1.8984375
- ffn_gain: bfloat16 [2048], replicated, may hold values from 0.099609375 to 1.8984375
- group_router: bfloat16 [2048, 2], replicated, may hold values from -0.125 to 0.125
- expert_router: bfloat16 [2048, 8], replicated, may hold values from -0.125 to 0.125
- route_experts: int32 [256, 4], P('ep'), may hold values from 0 to 7, as said below
- expert_gate: bfloat16 [8, 2048, 1024], P('ep', None, 'tp'), may hold values from -0.125 to 0.125
- expert_up: bfloat16 [8, 2048, 1024], P('ep', None, 'tp'), may hold values from -0.125 to 0.125
- expert_down: bfloat16 [8, 1024, 2048], P('ep', 'tp')
- dense_switch: bfloat16 [2048], replicated, may hold values from -0.125 to 0.125
- dense_gate: bfloat16 [2048, 2048], P('ep', 'tp'), may hold values from -0.125 to 0.125
- dense_up: bfloat16 [2048, 2048], P('ep', 'tp'), may hold values from -0.125 to 0.125
- dense_down: bfloat16 [2048, 2048], P('ep', 'tp')
- out_gain: bfloat16 [2048], P('tp'), may hold values from 0.099609375 to 1.8984375
Outputs:
- layer_out: bfloat16 [256, 2048], P('ep', 'tp')
- new_state: float32 [256, 8, 64, 128], P('ep', 'tp')
- new_conv: bfloat16 [256, 3, 3, 512], P('ep', None, None, 'tp')
Inputs may be any that keep to these rules, and one draw needn't show every extreme that they name: `route_experts`: each row names 4 different experts, all from one group of 4 consecutive expert numbers. Within each aligned block of 32 rows (the rows of one index of ep) no expert is named more than 32 times, and one expert, the same in every block, is named exactly 32 times in every block.
All inputs are finite; a program needn't handle non-finite values.
Results may differ from a plain program's by a relative error of at most 0.019.
Values may be sent and summed in bfloat16 or wider, within the bound.
A program may use at most 64 MiB of HBM per device.

v0:
```python
import jax
import jax.numpy as jnp
from jax import lax
from jax.sharding import PartitionSpec as P

norm_eps = 1e-06


def scaled_rows(values, gain):
    values = values.astype(jnp.float32)
    mean_square = jnp.mean(values * values, axis=-1, keepdims=True)
    return values * lax.rsqrt(mean_square + norm_eps) * gain.astype(jnp.float32)


def softmax_plain(logits):
    weights = jnp.exp(logits)
    return weights / jnp.sum(weights, axis=-1, keepdims=True)


def on_device(
    resid,
    mix_gain,
    proj_x,
    proj_z,
    proj_b,
    proj_c,
    proj_step,
    step_bias,
    decay_rate,
    conv_taps,
    conv_state,
    scan_state,
    inner_gain,
    proj_out,
    post_gain,
    ffn_gain,
    group_router,
    expert_router,
    route_experts,
    expert_gate,
    expert_up,
    expert_down,
    dense_switch,
    dense_gate,
    dense_up,
    dense_down,
    out_gain,
):
    tp_index = lax.axis_index("tp")
    seqs = resid.shape[0]
    width = resid.shape[1]
    quarter = width // lax.axis_size("tp")
    heads_here = scan_state.shape[1]
    head_dim = scan_state.shape[2]
    state_dim = scan_state.shape[3]
    channels = conv_state.shape[3]
    repeat = heads_here // (channels // state_dim)
    normed = scaled_rows(resid, mix_gain).astype(jnp.bfloat16)
    fresh = jnp.stack(
        [
            jnp.dot(normed, proj_x, preferred_element_type=jnp.float32),
            jnp.dot(normed, proj_b, preferred_element_type=jnp.float32),
            jnp.dot(normed, proj_c, preferred_element_type=jnp.float32),
        ],
        axis=1,
    ).astype(jnp.bfloat16)
    gate_z = jnp.dot(normed, proj_z, preferred_element_type=jnp.float32)
    step_all = jnp.dot(normed, proj_step, preferred_element_type=jnp.float32)
    step_raw = lax.dynamic_slice_in_dim(step_all, tp_index * heads_here, heads_here, 1)
    history = jnp.concatenate([conv_state, fresh[:, :, None, :]], axis=2)
    activated = jax.nn.silu(
        jnp.sum(history.astype(jnp.float32) * conv_taps.astype(jnp.float32)[None], axis=2)
    )
    xs_heads = activated[:, 0].reshape(seqs, heads_here, head_dim)
    b_heads = jnp.repeat(activated[:, 1].reshape(seqs, -1, state_dim), repeat, axis=1)
    c_heads = jnp.repeat(activated[:, 2].reshape(seqs, -1, state_dim), repeat, axis=1)
    step = jax.nn.softplus(step_raw + step_bias)
    keep = jnp.exp(-decay_rate * step)
    driven = step[:, :, None] * xs_heads
    new_state = keep[:, :, None, None] * scan_state + driven[:, :, :, None] * b_heads[:, :, None, :]
    read = jnp.sum(new_state * c_heads[:, :, None, :], axis=3).reshape(seqs, channels)
    gated = (read * jax.nn.silu(gate_z) * inner_gain.astype(jnp.float32)).astype(jnp.bfloat16)
    mixed = lax.psum(
        jnp.dot(gated, proj_out, preferred_element_type=jnp.float32).astype(jnp.bfloat16), "tp"
    ).astype(jnp.float32)
    stream = (resid.astype(jnp.float32) + scaled_rows(mixed, post_gain)).astype(jnp.bfloat16)
    feed = scaled_rows(stream, ffn_gain).astype(jnp.bfloat16)
    feed_quarter = lax.dynamic_slice_in_dim(feed, tp_index * quarter, quarter, 1)
    expert_count = expert_router.shape[1]
    group_size = expert_count // group_router.shape[1]
    pick_count = route_experts.shape[1]
    group_prob = softmax_plain(jnp.dot(feed, group_router, preferred_element_type=jnp.float32))
    expert_logits = jnp.dot(feed, expert_router, preferred_element_type=jnp.float32)
    matches = route_experts[:, :, None] == jnp.arange(expert_count, dtype=jnp.int32)[None, None, :]
    pick_logits = jnp.sum(jnp.where(matches, expert_logits[:, None, :], 0.0), axis=2)
    chosen_group = route_experts[:, 0] // group_size
    group_ids = jnp.arange(group_router.shape[1], dtype=jnp.int32)
    group_weight = jnp.sum(
        jnp.where(chosen_group[:, None] == group_ids[None, :], group_prob, 0.0), axis=1
    )
    pick_weight = softmax_plain(pick_logits) * group_weight[:, None]
    capacity = 2 * seqs * pick_count // expert_count
    flat_picks = route_experts.reshape(-1)
    one_hot = (flat_picks[:, None] == jnp.arange(expert_count, dtype=jnp.int32)[None, :]).astype(
        jnp.int32
    )
    slot = jnp.sum((jnp.cumsum(one_hot, axis=0) - one_hot) * one_hot, axis=1)
    target = flat_picks * capacity + slot
    repeated = jnp.repeat(feed, pick_count, axis=0)
    outgoing = jnp.zeros((expert_count * capacity, width), jnp.bfloat16).at[target].set(repeated)
    outgoing = outgoing.reshape(expert_count, capacity, width)
    arrived = lax.all_to_all(outgoing, "ep", split_axis=0, concat_axis=0, tiled=True)
    sources = arrived.shape[0]
    items = arrived.shape[1]
    rows = arrived.reshape(sources * items, width)
    gate_value = jnp.dot(rows, expert_gate[0], preferred_element_type=jnp.float32)
    up_value = jnp.dot(rows, expert_up[0], preferred_element_type=jnp.float32)
    hidden = (jax.nn.silu(gate_value) * up_value).astype(jnp.bfloat16)
    result = jnp.dot(hidden, expert_down[0], preferred_element_type=jnp.float32).reshape(
        sources, items, width
    )
    summed = lax.psum_scatter(result.astype(jnp.bfloat16), "tp", scatter_dimension=2, tiled=True)
    returned = lax.all_to_all(summed, "ep", split_axis=0, concat_axis=0, tiled=True)
    fetched = returned.reshape(expert_count * capacity, quarter)[target].reshape(
        seqs, pick_count, quarter
    )
    routed = jnp.sum(fetched.astype(jnp.float32) * pick_weight[:, :, None], axis=1)
    gate_piece = jnp.einsum(
        "sd,cd->sc",
        feed_quarter,
        lax.all_gather(dense_gate, "ep", axis=0, tiled=True),
        preferred_element_type=jnp.float32,
    )
    up_piece = jnp.einsum(
        "sd,cd->sc",
        feed_quarter,
        lax.all_gather(dense_up, "ep", axis=0, tiled=True),
        preferred_element_type=jnp.float32,
    )
    gate_sum = gate_piece
    up_sum = up_piece
    gate_sum, up_sum = (
        lax.psum(gate_sum.astype(jnp.bfloat16), "tp").astype(jnp.float32),
        lax.psum(up_sum.astype(jnp.bfloat16), "tp").astype(jnp.float32),
    )
    dense_hidden = (jax.nn.silu(gate_sum) * up_sum).astype(jnp.bfloat16)
    dense_out = jnp.dot(
        dense_hidden,
        lax.all_gather(dense_down, "ep", axis=0, tiled=True),
        preferred_element_type=jnp.float32,
    )
    switch = jax.nn.sigmoid(jnp.dot(feed, dense_switch, preferred_element_type=jnp.float32))
    combined = routed + switch[:, None] * dense_out
    total_square = lax.psum(jnp.sum(combined * combined, axis=1), "tp")
    scale = lax.rsqrt(total_square / width + norm_eps)
    stream_part = lax.dynamic_slice_in_dim(stream, tp_index * quarter, quarter, 1).astype(
        jnp.float32
    )
    layer_out = (stream_part + combined * scale[:, None] * out_gain.astype(jnp.float32)).astype(
        jnp.bfloat16
    )
    new_conv = history[:, :, 1:, :]
    return (layer_out, new_state, new_conv)


def solution(mesh):
    placed = (
        P("ep", None),
        P(),
        P(None, "tp"),
        P(None, "tp"),
        P(None, "tp"),
        P(None, "tp"),
        P(),
        P("tp"),
        P("tp"),
        P(None, None, "tp"),
        P("ep", None, None, "tp"),
        P("ep", "tp", None, None),
        P("tp"),
        P("tp", None),
        P(),
        P(),
        P(),
        P(),
        P("ep", None),
        P("ep", None, "tp"),
        P("ep", None, "tp"),
        P("ep", "tp", None),
        P(),
        P("ep", "tp"),
        P("ep", "tp"),
        P("ep", "tp"),
        P("tp"),
    )
    return jax.shard_map(
        on_device,
        mesh=mesh,
        in_specs=placed,
        out_specs=(P("ep", "tp"), P("ep", "tp", None, None), P("ep", None, None, "tp")),
        check_vma=False,
    )
```

profile of v0, /device:TPU:0, one launch (start us, length us, event | category | flops | bytes accessed | tf_op | source)
XLA Modules:
  0.0 219.6 jit_solution(17043526989973223200)
XLA Ops:
  8.0 0.0 copy-start
  8.1 0.0 all-reduce.4.cloned.1.call-start
  8.1 0.8 convert_element_type.91
  9.0 1.1 fusion.24
  10.1 1.4 fusion.2
  11.4 1.4 fusion.3
  12.8 1.4 fusion.4
  14.2 0.9 multiply_reduce_fusion.2
  15.2 0.1 reshape_squeeze.3
  15.3 1.0 fusion.48
  16.3 0.1 multiply_exponential_fusion
  16.4 0.1 copy.43
  16.5 0.1 copy.42
  16.6 0.1 broadcast_multiply_fusion
  16.7 0.0 copy-start.15
  16.7 2.1 multiply_reduce_fusion
  18.8 0.1 reshape.185
  18.9 2.3 %convolution_convert_fusion.3 = bf16[32,2048]{1,0:T(8,128)(2,1)} fusion(bf16[128,2048]{1,0:T(8,128)(2,1)} %param.40, f32[32,128]{1,0:T(8,128)S(1)} %reshape.185, f32[128]{0:T(128)S(1)} %convert_element_type.95, bf16[2048,128]{1,0:T(8,128)(2,1)} %param.30, bf16[32,2048]{1,0:T(8,128)(2,1)S(1)} %copy-done.1, f32[2048]{0:T(1024)S(1)} %convert_element_type.91, ...), kind=kOutput, calls=%fused_computation.5 | convolution fusion | flops 33910784 | bytes 1335936 | tf_op jit(solution)/shard_map/dot_general | solution.py:84
  21.3 0.0 all-reduce.4.cloned.1.call-update
  21.3 0.0 all-gather.6.cloned.1.call-start
  21.3 0.5 all-gather.6.cloned.1.call-update
  21.9 0.0 reduce-scatter.2.cloned.1.call-start
  21.9 0.1 copy.45
  22.0 0.1 eq.43
  22.2 0.1 fusion.31
  22.2 0.2 reduce_window_sum.11
  22.4 0.2 select_reduce_fusion
  22.6 0.1 copy.44
  22.7 0.1 mul.252
  22.8 33.1 %all-reduce.4.cloned.1.call-done = bf16[32,2048]{1,0:T(8,128)(2,1)} async-done(((bf16[32,2048]{1,0:T(8,128)(2,1)}), bf16[32,2048]{1,0:T(8,128)(2,1)}) %all-reduce.4.cloned.1.call-update) | async-done | bytes 131088 | tf_op jit(solution)/shard_map/psum | solution.py:83
  55.9 1.0 fusion.15
  57.0 1.2 fusion.17
  58.2 0.1 fusion.19
  58.3 0.2 broadcast_in_dim.14
  58.5 0.9 reshape.203
  59.4 2.2 %scatter_custom_fusion = bf16[256,2048]{1,0:T(8,128)(2,1)S(1)} fusion(s32[128]{0:T(128)S(1)} %fusion.39, bf16[128,2048]{1,0:T(8,128)(2,1)} %reshape.203, bf16[]{:T(256)} %constant.57.clone.1), kind=kCustom, calls=%fused_computation.28 | custom fusion | bytes 1049088 | tf_op jit(solution)/shard_map/scatter | solution.py:110
  61.7 36.1 %all_to_all.10 = bf16[8,32,2048]{2,1,0:T(8,128)(2,1)S(1)} all-to-all(bf16[8,32,2048]{2,1,0:T(8,128)(2,1)S(1)} %bitcast.63), channel_id=1, replica_groups=mesh['ep'=8,'tp'=4] {'ep'}, dimensions={0} | all-to-all | bytes 2097152 | tf_op jit(solution)/shard_map/all_to_all | solution.py:112
  97.7 0.4 fusion.11
  98.2 0.4 fusion
  98.7 1.4 convolution_convert_fusion
  100.1 0.0 reduce-scatter.2.cloned.1.call-update
  100.2 0.0 all-gather.4.cloned.1.call-start
  100.2 0.5 all-gather.4.cloned.1.call-update
  100.7 0.0 all-gather.8.cloned.1.call-start
  100.8 0.5 all-gather.8.cloned.1.call-update
  101.4 0.6 slice.31
  102.0 0.1 fusion.57
  102.2 0.2 fusion.56
  102.4 0.1 fusion.8
  102.6 3.1 %convolution_convert_fusion.1 = bf16[32,2048]{1,0:T(8,128)(2,1)} fusion(bf16[2048,512]{1,0:T(8,128)(2,1)} %all-gather.6.cloned.1.call-done, bf16[32,2048]{1,0:T(8,128)(2,1)S(1)} %fusion.19, s32[]{:T(128)S(6)} %select_n.38), kind=kOutput, calls=%fused_computation.3 | convolution fusion | flops 67174400 | bytes 2260996 | tf_op jit(solution)/shard_map/sd,cd->sc/dot_general | solution.py:134
  105.7 17.5 %reduce-scatter.2.cloned.1.call-done = bf16[8,32,512]{2,1,0:T(8,128)(2,1)} async-done(((bf16[8,32,2048]{2,1,0:T(8,128)(2,1)}), bf16[8,32,512]{2,1,0:T(8,128)(2,1)}) %reduce-scatter.2.cloned.1.call-update) | async-done | bytes 262160 | tf_op jit(solution)/shard_map/reduce_scatter | solution.py:122
  123.2 5.5 %all-to-all-start.1 = ((bf16[8,32,512]{2,1,0:T(8,128)(2,1)}), bf16[8,32,512]{2,1,0:T(8,128)(2,1)S(1)}, u32[]{:S(2)}, u32[]{:S(2)}) async-start(bf16[8,32,512]{2,1,0:T(8,128)(2,1)} %reduce-scatter.2.cloned.1.call-done), calls=%async_computation.2 | async-start | bytes 524288 | tf_op jit(solution)/shard_map/all_to_all | solution.py:123
  128.8 0.0 all-reduce.6.cloned.1.call-start
  128.8 24.4 %all-gather.4.cloned.1.call-done = bf16[2048,512]{1,0:T(8,128)(2,1)} async-done(((bf16[256,512]{1,0:T(8,128)(2,1)}), bf16[2048,512]{1,0:T(8,128)(2,1)}) %all-gather.4.cloned.1.call-update) | async-done | bytes 2097168 | tf_op jit(solution)/shard_map/all_gather | solution.py:131
  153.2 3.0 %convolution_convert_fusion.2 = bf16[32,2048]{1,0:T(8,128)(2,1)} fusion(bf16[2048,512]{1,0:T(8,128)(2,1)} %all-gather.4.cloned.1.call-done, bf16[32,2048]{1,0:T(8,128)(2,1)S(1)} %fusion.19, s32[]{:T(128)S(6)} %select_n.38), kind=kOutput, calls=%fused_computation.4 | convolution fusion | flops 67174400 | bytes 2260996 | tf_op jit(solution)/shard_map/sd,cd->sc/dot_general | solution.py:128
  156.2 0.0 all-reduce.6.cloned.1.call-update
  156.2 0.1 copy.46
  156.3 0.8 gather_fusion
  157.2 0.1 reshape.190
  157.3 0.2 multiply_reduce_fusion.1
  157.5 46.1 %all-gather.8.cloned.1.call-done = bf16[2048,512]{1,0:T(8,128)(2,1)} async-done(((bf16[256,512]{1,0:T(8,128)(2,1)}), bf16[2048,512]{1,0:T(8,128)(2,1)}) %all-gather.8.cloned.1.call-update) | async-done | bytes 2097168 | tf_op jit(solution)/shard_map/all_gather | solution.py:149
  203.6 2.3 %multiply_reduce_fusion.3 = (f32[32]{0:T(128)S(1)}, f32[32,512]{1,0:T(8,128)S(1)}) fusion(f32[32,512]{1,0:T(8,128)S(1)} %multiply_reduce_fusion.1, bf16[2048,512]{1,0:T(8,128)(2,1)} %all-gather.8.cloned.1.call-done, bf16[32,2048]{1,0:T(8,128)(2,1)} %get-tuple-element.3, bf16[32,2048]{1,0:T(8,128)(2,1)} %get-tuple-element.4, f32[32]{0:T(128)S(1)} %fusion.8), kind=kOutput, calls=%fused_computation.58 | convolution fusion | flops 67698656 | bytes 2490624 | tf_op jit(solution)/shard_map/dot_general | solution.py:147
  205.9 5.7 %psum.31 = f32[32]{0:T(128)S(1)} all-reduce(f32[32]{0:T(128)S(1)} %get-tuple-element.18), channel_id=1, replica_groups=mesh['ep'=8,'tp'=4] {'tp'}, use_global_device_ids=true, to_apply=%region_18.19 | all-reduce | flops 32 | bytes 256 | tf_op jit(solution)/shard_map/psum | solution.py:154
  211.5 0.7 add_convert_fusion
  (54 shorter events, 0.3 us)
Async XLA Ops:
  8.0 90.7 %copy-start = (bf16[1,256,2048]{2,1,0:T(8,128)(2,1)S(1)}, bf16[1,256,2048]{2,1,0:T(8,128)(2,1)}, u32[]{:S(2)}) copy-start(bf16[1,256,2048]{2,1,0:T(8,128)(2,1)} %param.48) | copy-start | bytes 3145732
  8.0 7.3 %copy-start.1 = (bf16[32,2048]{1,0:T(8,128)(2,1)S(1)}, bf16[32,2048]{1,0:T(8,128)(2,1)}, u32[]{:S(2)}) copy-start(bf16[32,2048]{1,0:T(8,128)(2,1)} %param.27) | copy-start | bytes 393220
  8.0 6.2 %copy-start.9 = (bf16[3,4,128]{2,1,0:T(4,128)(2,1)S(1)}, bf16[3,4,128]{2,1,0:T(4,128)(2,1)}, u32[]{:S(2)}) copy-start(bf16[3,4,128]{2,1,0:T(4,128)(2,1)} %param.36) | copy-start | bytes 9220
  8.0 8.2 %copy-start.14 = (f32[2]{0:T(128)S(1)}, f32[2]{0:T(128)}, u32[]{:S(2)}) copy-start(f32[2]{0:T(128)} %param.35) | copy-start | bytes 28
  8.0 8.2 %copy-start.11 = (f32[2]{0:T(128)S(1)}, f32[2]{0:T(128)}, u32[]{:S(2)}) copy-start(f32[2]{0:T(128)} %param.34) | copy-start | bytes 28
  8.1 8.6 %copy-start.2 = (f32[32,2,64,128]{3,2,1,0:T(8,128)S(1)}, f32[32,2,64,128]{3,2,1,0:T(8,128)}, u32[]{:S(2)}) copy-start(f32[32,2,64,128]{3,2,1,0:T(8,128)} %param.38) | copy-start | bytes 6291460
  8.1 47.9 %all-reduce.4.cloned.1.call-start = ((), (), s32[]{:S(2)}) async-start(), calls=%async_computation.3 | async-start | bytes 262144 | tf_op jit(solution)/shard_map/psum | solution.py:83
  16.7 2.2 %copy-start.15 = (bf16[128]{0:T(256)(128)(2,1)S(1)}, bf16[128]{0:T(256)(128)(2,1)}, u32[]{:S(2)}) copy-start(bf16[128]{0:T(256)(128)(2,1)} %param.39) | copy-start | bytes 772
  16.7 5.2 %copy-start.5 = (s32[32,4]{0,1:T(4,128)S(1)}, s32[32,4]{0,1:T(4,128)}, u32[]{:S(2)}) copy-start(s32[32,4]{0,1:T(4,128)} %param.45) | copy-start | bytes 1540
  16.7 5.3 %copy-start.6 = (bf16[2048]{0:T(1024)(128)(2,1)S(1)}, bf16[2048]{0:T(1024)(128)(2,1)}, u32[]{:S(2)}) copy-start(bf16[2048]{0:T(1024)(128)(2,1)} %param.41) | copy-start | bytes 12292
  16.7 5.3 %copy-start.7 = (bf16[2048]{0:T(1024)(128)(2,1)S(1)}, bf16[2048]{0:T(1024)(128)(2,1)}, u32[]{:S(2)}) copy-start(bf16[2048]{0:T(1024)(128)(2,1)} %param.42) | copy-start | bytes 12292
  21.3 81.3 %all-gather.6.cloned.1.call-start = ((), (), s32[]{:S(2)}) async-start(), calls=%async_computation.6 | async-start | bytes 2359296 | tf_op jit(solution)/shard_map/all_gather | solution.py:137
  21.9 101.4 %reduce-scatter.2.cloned.1.call-start = ((), (), s32[]{:S(2)}) async-start(), calls=%async_computation.4 | async-start | bytes 1310720 | tf_op jit(solution)/shard_map/reduce_scatter | solution.py:122
  58.5 39.2 %copy-start.3 = (bf16[1,2048,256]{2,1,0:T(8,128)(2,1)S(1)}, bf16[1,2048,256]{2,1,0:T(8,128)(2,1)}, u32[]{:S(2)}) copy-start(bf16[1,2048,256]{2,1,0:T(8,128)(2,1)} %param.46) | copy-start | bytes 3145732
  61.6 36.5 %copy-start.12 = (bf16[1,2048,256]{2,1,0:T(8,128)(2,1)S(1)}, bf16[1,2048,256]{2,1,0:T(8,128)(2,1)}, u32[]{:S(2)}) copy-start(bf16[1,2048,256]{2,1,0:T(8,128)(2,1)} %param.47) | copy-start | bytes 3145732
  98.6 2.7 %copy-start.8 = (bf16[2048]{0:T(1024)(128)(2,1)S(1)}, bf16[2048]{0:T(1024)(128)(2,1)}, u32[]{:S(2)}) copy-start(bf16[2048]{0:T(1024)(128)(2,1)} %param.49) | copy-start | bytes 12292
  98.6 2.7 %copy-start.10 = (bf16[512]{0:T(512)(128)(2,1)S(1)}, bf16[512]{0:T(512)(128)(2,1)}, u32[]{:S(2)}) copy-start(bf16[512]{0:T(512)(128)(2,1)} %param.53) | copy-start | bytes 3076
  98.7 3.4 %copy-start.4 = (bf16[2048,8]{0,1:T(8,128)(2,1)S(1)}, bf16[2048,8]{0,1:T(8,128)(2,1)}, u32[]{:S(2)}) copy-start(bf16[2048,8]{0,1:T(8,128)(2,1)} %param.44) | copy-start | bytes 98308
  98.7 3.6 %copy-start.13 = (bf16[2048,2]{0,1:T(2,128)(2,1)S(1)}, bf16[2048,2]{0,1:T(2,128)(2,1)}, u32[]{:S(2)}) copy-start(bf16[2048,2]{0,1:T(2,128)(2,1)} %param.43) | copy-start | bytes 24580
  100.2 53.1 %all-gather.4.cloned.1.call-start = ((), (), s32[]{:S(2)}) async-start(), calls=%async_computation.5 | async-start | bytes 2359296 | tf_op jit(solution)/shard_map/all_gather | solution.py:131
  100.7 102.8 %all-gather.8.cloned.1.call-start = ((), (), s32[]{:S(2)}) async-start(), calls=%async_computation.7 | async-start | bytes 2359296 | tf_op jit(solution)/shard_map/all_gather | solution.py:149
  123.2 33.1 %all-to-all-start.1 = ((bf16[8,32,512]{2,1,0:T(8,128)(2,1)}), bf16[8,32,512]{2,1,0:T(8,128)(2,1)S(1)}, u32[]{:S(2)}, u32[]{:S(2)}) async-start(bf16[8,32,512]{2,1,0:T(8,128)(2,1)} %reduce-scatter.2.cloned.1.call-done), calls=%async_computation.2 | async-start | bytes 524288 | tf_op jit(solution)/shard_map/all_to_all | solution.py:123
  128.8 74.8 %all-reduce.6.cloned.1.call-start = ((), (), s32[]{:S(2)}) async-start(), calls=%async_computation.8 | async-start | bytes 524288 | tf_op jit(solution)/shard_map/psum | solution.py:144
Sparse Core Ops, SparseCore 0:
  21.4 34.4 all-reduce.3
  100.3 22.9 reduce-scatter.1
  156.3 31.6 all-reduce.5
Sparse Core Ops, SparseCore 1:
  23.9 59.7 all-gather.5
  102.8 50.4 all-gather.3
  155.2 48.3 all-gather.7
where the time goes:
time: 220 us
  waiting for transfers between devices  123 us (56%)
  blocking collectives  41.7 us (19%)
  matrix products  18.6 us (8%)
  between operations  15.9 us (7%)
  other arithmetic  8.99 us (4%)
  local copies, waits for them, and re-layouts  5.86 us (3%)
  starting transfers between devices  5.78 us (3%)
    all_gather x1, waiting for transfers between devices, on_device(): lax.all_gather(dense_down, 'ep', axis=0, tiled=True)  46.1 us
    all_to_all x1, blocking collectives, on_device(): lax.all_to_all(outgoing, 'ep', split_axis=0, concat_axis=0, tiled=True)  36.1 us
    psum x1, waiting for transfers between devices, on_device(): lax.psum(jnp.dot(gated, proj_out, preferred_element_type=jnp.float32).ast...  33.1 us
    all_gather x1, waiting for transfers between devices, on_device(): lax.all_gather(dense_gate, 'ep', axis=0, tiled=True)  24.4 us
    reduce_scatter x1, waiting for transfers between devices, on_device(): lax.psum_scatter(result.astype(jnp.bfloat16), 'tp', scatter_dimension=2,...  17.5 us
    psum x1, blocking collectives, on_device(): total_square = lax.psum(jnp.sum(combined * combined, axis=1), 'tp')  5.67 us
    all_to_all x1, starting transfers between devices, on_device(): lax.all_to_all(summed, 'ep', split_axis=0, concat_axis=0, tiled=True)  5.53 us
  transfers between devices with their start and end apart: 7, of which 4 were waited for; matrix products, arithmetic and copies ran while one was open for 8% of the time, Pallas kernels for 0%

commit v1 on v0

--- a/solution.py
+++ b/solution.py
@@ -125,12 +125,23 @@
         seqs, pick_count, quarter
     )
     routed = jnp.sum(fetched.astype(jnp.float32) * pick_weight[:, :, None], axis=1)
-    gate_piece = jnp.einsum(
-        "sd,cd->sc",
-        feed_quarter,
-        lax.all_gather(dense_gate, "ep", axis=0, tiled=True),
-        preferred_element_type=jnp.float32,
-    )
+    ways, here, step_2 = (lax.axis_size("ep"), lax.axis_index("ep"), dense_gate.shape[0])
+    earlier, later = ([], [])
+    going_up = going_down = dense_gate
+    for far in range(ways // 2 + 1):
+        earlier.append(
+            jnp.einsum("sd,cd->sc", feed_quarter, going_up, preferred_element_type=jnp.float32)
+        )
+        if 0 < far < ways - ways // 2:
+            later.append(
+                jnp.einsum(
+                    "sd,cd->sc", feed_quarter, going_down, preferred_element_type=jnp.float32
+                )
+            )
+        going_up = lax.ppermute(going_up, "ep", [(d, (d + 1) % ways) for d in range(ways)])
+        going_down = lax.ppermute(going_down, "ep", [(d, (d - 1) % ways) for d in range(ways)])
+    line = jnp.concatenate([*earlier[::-1], *later], axis=1)
+    gate_piece = jnp.roll(line, (here - ways // 2) * earlier[0].shape[1], axis=1)
     up_piece = jnp.einsum(
         "sd,cd->sc",
         feed_quarter,

time: 220 us -> 232 us (1.055)
  starting transfers between devices: 5.78 us -> 19.1 us
  waiting for transfers between devices: 123 us -> 129 us
  blocking collectives: 41.7 us -> 35.9 us
    ppermute x0 -> x7, waiting for transfers between devices: none -> 43.3 us  [the longest x4 39.7 us: on_device(): lax.ppermute(going_up, 'ep', [(d, (d + 1) % ways) for d in range(ways)])]
    all_gather x1 -> x0, waiting for transfers between devices: 24.4 us -> none  [on_device(): lax.all_gather(dense_gate, 'ep', axis=0, tiled=True)]
    reduce_scatter x1, waiting for transfers between devices: 17.5 us -> 0.01 us  [on_device(): lax.psum_scatter(result.astype(jnp.bfloat16), 'tp', scatter_dimension=2,...]
    ppermute x0 -> x7, starting transfers between devices: none -> 15.5 us  [the longest x3 8.34 us: on_device(): lax.ppermute(going_down, 'ep', [(d, (d - 1) % ways) for d in range(ways)])]
    all_to_all x1, blocking collectives: 36.1 us -> 30.2 us  [on_device(): lax.all_to_all(outgoing, 'ep', split_axis=0, concat_axis=0, tiled=True)]
    all_gather x1, waiting for transfers between devices: 0.01 us -> 4.8 us  [on_device(): lax.all_gather(dense_up, 'ep', axis=0, tiled=True)]
  transfers between devices with their start and end apart: 7 -> 13, of which waited for: 4 -> 10; matrix products, arithmetic and copies ran while one was open for 8% -> 4% of each run, Pallas kernels for 0% -> 0%
where the time goes in v1:
time: 232 us
  waiting for transfers between devices  129 us (56%)
  blocking collectives  35.9 us (15%)
  starting transfers between devices  19.1 us (8%)
  matrix products  16.9 us (7%)
  between operations  15.7 us (7%)
  other arithmetic  8.98 us (4%)
  local copies, waits for them, and re-layouts  6.56 us (3%)
    all_gather x1, waiting for transfers between devices, on_device(): lax.all_gather(dense_down, 'ep', axis=0, tiled=True)  45.9 us
    ppermute x4, waiting for transfers between devices, on_device(): lax.ppermute(going_up, 'ep', [(d, (d + 1) % ways) for d in range(ways)])  39.7 us
    psum x1, waiting for transfers between devices, on_device(): lax.psum(jnp.dot(gated, proj_out, preferred_element_type=jnp.float32).ast...  33.8 us
    all_to_all x1, blocking collectives, on_device(): lax.all_to_all(outgoing, 'ep', split_axis=0, concat_axis=0, tiled=True)  30.2 us
    ppermute x3, starting transfers between devices, on_device(): lax.ppermute(going_down, 'ep', [(d, (d - 1) % ways) for d in range(ways)])  8.34 us
    ppermute x4, starting transfers between devices, on_device(): lax.ppermute(going_up, 'ep', [(d, (d + 1) % ways) for d in range(ways)])  7.18 us
    psum x1, blocking collectives, on_device(): total_square = lax.psum(jnp.sum(combined * combined, axis=1), 'tp')  5.67 us
    all_gather x1, waiting for transfers between devices, on_device(): lax.all_gather(dense_up, 'ep', axis=0, tiled=True)  4.8 us
  transfers between devices with their start and end apart: 13, of which 10 were waited for; matrix products, arithmetic and copies ran while one was open for 4% of the time, Pallas kernels for 0%

profile of v1, /device:TPU:0, one launch (start us, length us, event | category | flops | bytes accessed | tf_op | source)
XLA Modules:
  0.0 231.7 jit_solution(6356211131729690227)
XLA Ops:
  8.1 0.8 convert_element_type.91
  9.0 1.1 fusion.24
  10.1 1.4 fusion.2
  11.4 1.4 fusion.3
  12.8 1.4 fusion.4
  14.2 0.9 multiply_reduce_fusion.2
  15.3 1.0 fusion.52
  16.6 0.1 broadcast_multiply_fusion
  16.7 2.1 multiply_reduce_fusion
  18.8 0.1 reshape.185
  18.9 2.3 %convolution_convert_fusion.2 = bf16[32,2048]{1,0:T(8,128)(2,1)} fusion(bf16[128,2048]{1,0:T(8,128)(2,1)} %param.40, f32[32,128]{1,0:T(8,128)S(1)} %reshape.185, f32[128]{0:T(128)S(1)} %convert_element_type.95, bf16[2048,128]{1,0:T(8,128)(2,1)} %param.30, bf16[32,2048]{1,0:T(8,128)(2,1)S(1)} %copy-done.1, f32[2048]{0:T(1024)S(1)} %convert_element_type.91, ...), kind=kOutput, calls=%fused_computation.4 | convolution fusion | flops 33910784 | bytes 1335936 | tf_op jit(solution)/shard_map/dot_general | solution.py:84
  21.4 0.1 eq.46
  21.5 0.1 fusion.31
  21.6 0.2 reduce_window_sum.11
  21.8 0.2 select_reduce_fusion
  22.1 0.1 mul.255
  22.2 33.8 %all-reduce.4.cloned.1.call-done = bf16[32,2048]{1,0:T(8,128)(2,1)} async-done(((bf16[32,2048]{1,0:T(8,128)(2,1)}), bf16[32,2048]{1,0:T(8,128)(2,1)}) %all-reduce.4.cloned.1.call-update) | async-done | bytes 131088 | tf_op jit(solution)/shard_map/psum | solution.py:83
  56.0 1.0 fusion.15
  57.0 1.2 fusion.17
  58.2 0.1 fusion.19
  58.3 0.2 broadcast_in_dim.14
  58.6 0.9 reshape.203
  59.5 2.2 scatter_custom_fusion
  61.7 30.2 %all_to_all.10 = bf16[8,32,2048]{2,1,0:T(8,128)(2,1)S(1)} all-to-all(bf16[8,32,2048]{2,1,0:T(8,128)(2,1)S(1)} %bitcast.70), channel_id=1, replica_groups=mesh['ep'=8,'tp'=4] {'ep'}, dimensions={0} | all-to-all | bytes 2097152 | tf_op jit(solution)/shard_map/all_to_all | solution.py:112
  91.9 0.4 fusion.11
  92.4 0.4 fusion
  92.9 1.4 convolution_convert_fusion
  94.4 0.5 all-gather.3.cloned.1.call-update
  95.0 1.5 collective-permute-start
  96.4 3.3 %collective-permute-start.4 = (bf16[256,512]{1,0:T(8,128)(2,1)S(1)}, bf16[256,512]{1,0:T(8,128)(2,1)S(1)}, u32[]{:S(2)}, u32[]{:S(2)}) collective-permute-start(bf16[256,512]{1,0:T(8,128)(2,1)S(1)} %copy-done.4), channel_id=1, source_target_pairs={{0,28},{4,0},{8,4},{12,8},{16,12},{20,16},{24,20},{28,24},{1,29},{... | collective-permute-start | bytes 786440 | tf_op jit(solution)/shard_map/ppermute | solution.py:142
  99.8 9.6 %collective-permute-done = bf16[256,512]{1,0:T(8,128)(2,1)S(1)} collective-permute-done((bf16[256,512]{1,0:T(8,128)(2,1)S(1)}, bf16[256,512]{1,0:T(8,128)(2,1)S(1)}, u32[]{:S(2)}, u32[]{:S(2)}) %collective-permute-start) | collective-permute-done | bytes 262176 | tf_op jit(solution)/shard_map/ppermute | solution.py:141
  109.4 2.5 %collective-permute-start.1 = (bf16[256,512]{1,0:T(8,128)(2,1)S(1)}, bf16[256,512]{1,0:T(8,128)(2,1)S(1)}, u32[]{:S(2)}, u32[]{:S(2)}) collective-permute-start(bf16[256,512]{1,0:T(8,128)(2,1)S(1)} %collective-permute-done), channel_id=1, source_target_pairs={{0,4},{4,8},{8,12},{12,16},{16,20},{20,24},{24,28},{28,0},{1,5},{5... | collective-permute-start | bytes 786440 | tf_op jit(solution)/shard_map/ppermute | solution.py:141
  111.9 0.6 slice.31
  112.6 0.1 fusion.61
  112.7 10.1 %collective-permute-done.1 = bf16[256,512]{1,0:T(8,128)(2,1)S(1)} collective-permute-done((bf16[256,512]{1,0:T(8,128)(2,1)S(1)}, bf16[256,512]{1,0:T(8,128)(2,1)S(1)}, u32[]{:S(2)}, u32[]{:S(2)}) %collective-permute-start.1) | collective-permute-done | bytes 262176 | tf_op jit(solution)/shard_map/ppermute | solution.py:141
  122.8 0.2 fusion.60
  123.1 4.8 %collective-permute-start.5 = (bf16[256,512]{1,0:T(8,128)(2,1)S(1)}, bf16[256,512]{1,0:T(8,128)(2,1)S(1)}, u32[]{:S(2)}, u32[]{:S(2)}) collective-permute-start(bf16[256,512]{1,0:T(8,128)(2,1)S(1)} %collective-permute-done.4), channel_id=1, source_target_pairs={{0,28},{4,0},{8,4},{12,8},{16,12},{20,16},{24,20},{28,24},{1,29},{... | collective-permute-start | bytes 786440 | tf_op jit(solution)/shard_map/ppermute | solution.py:142
  127.8 10.0 %collective-permute-done.2 = bf16[256,512]{1,0:T(8,128)(2,1)S(1)} collective-permute-done((bf16[256,512]{1,0:T(8,128)(2,1)S(1)}, bf16[256,512]{1,0:T(8,128)(2,1)S(1)}, u32[]{:S(2)}, u32[]{:S(2)}) %collective-permute-start.2) | collective-permute-done | bytes 262176 | tf_op jit(solution)/shard_map/ppermute | solution.py:141
  137.9 3.2 %collective-permute-start.3 = (bf16[256,512]{1,0:T(8,128)(2,1)S(1)}, bf16[256,512]{1,0:T(8,128)(2,1)S(1)}, u32[]{:S(2)}, u32[]{:S(2)}) collective-permute-start(bf16[256,512]{1,0:T(8,128)(2,1)S(1)} %collective-permute-done.2), channel_id=1, source_target_pairs={{0,4},{4,8},{8,12},{12,16},{16,20},{20,24},{24,28},{28,0},{1,5},{5... | collective-permute-start | bytes 786440 | tf_op jit(solution)/shard_map/ppermute | solution.py:141
  141.1 0.1 fusion.8
  141.3 1.3 collective-permute-done.5
  142.5 0.3 collective-permute-start.6
  142.8 9.9 %collective-permute-done.3 = bf16[256,512]{1,0:T(8,128)(2,1)S(1)} collective-permute-done((bf16[256,512]{1,0:T(8,128)(2,1)S(1)}, bf16[256,512]{1,0:T(8,128)(2,1)S(1)}, u32[]{:S(2)}, u32[]{:S(2)}) %collective-permute-start.3) | collective-permute-done | bytes 262176 | tf_op jit(solution)/shard_map/ppermute | solution.py:141
  152.7 0.2 constant_dynamic-update-slice_fusion.15
  152.8 0.2 constant_dynamic-update-slice_fusion.14
  153.0 0.2 constant_dynamic-update-slice_fusion.13
  153.2 0.2 constant_dynamic-update-slice_fusion.12
  153.4 0.2 constant_dynamic-update-slice_fusion.11
  153.6 0.2 constant_dynamic-update-slice_fusion.10
  153.8 0.2 constant_dynamic-update-slice_fusion.9
  154.0 2.3 %collective-permute-done.6 = bf16[256,512]{1,0:T(8,128)(2,1)S(1)} collective-permute-done((bf16[256,512]{1,0:T(8,128)(2,1)S(1)}, bf16[256,512]{1,0:T(8,128)(2,1)S(1)}, u32[]{:S(2)}, u32[]{:S(2)}) %collective-permute-start.6) | collective-permute-done | bytes 262176 | tf_op jit(solution)/shard_map/ppermute | solution.py:142
  156.3 0.2 constant_dynamic-update-slice_fusion.8
  156.6 0.7 dynamic-slice_convert_fusion
  157.3 3.4 %all-to-all-start.1 = ((bf16[8,32,512]{2,1,0:T(8,128)(2,1)}), bf16[8,32,512]{2,1,0:T(8,128)(2,1)S(1)}, u32[]{:S(2)}, u32[]{:S(2)}) async-start(bf16[8,32,512]{2,1,0:T(8,128)(2,1)} %reduce-scatter.2.cloned.1.call-done), calls=%async_computation.2 | async-start | bytes 524288 | tf_op jit(solution)/shard_map/all_to_all | solution.py:123
  160.7 4.8 %all-gather.3.cloned.1.call-done = bf16[2048,512]{1,0:T(8,128)(2,1)} async-done(((bf16[256,512]{1,0:T(8,128)(2,1)}), bf16[2048,512]{1,0:T(8,128)(2,1)}) %all-gather.3.cloned.1.call-update) | async-done | bytes 2097168 | tf_op jit(solution)/shard_map/all_gather | solution.py:148
  165.5 2.9 %convolution_convert_fusion.1 = bf16[32,2048]{1,0:T(8,128)(2,1)} fusion(bf16[2048,512]{1,0:T(8,128)(2,1)} %all-gather.3.cloned.1.call-done, bf16[32,2048]{1,0:T(8,128)(2,1)S(1)} %fusion.19, s32[]{:T(128)S(6)} %select_n.51), kind=kOutput, calls=%fused_computation.3 | convolution fusion | flops 67174400 | bytes 2260996 | tf_op jit(solution)/shard_map/sd,cd->sc/dot_general | solution.py:145
  168.6 0.2 all-to-all-done.1
  168.9 0.8 gather_fusion
  169.7 0.1 reshape.190
  169.8 0.2 multiply_reduce_fusion.1
  170.0 45.9 %all-gather.5.cloned.1.call-done = bf16[2048,512]{1,0:T(8,128)(2,1)} async-done(((bf16[256,512]{1,0:T(8,128)(2,1)}), bf16[2048,512]{1,0:T(8,128)(2,1)}) %all-gather.5.cloned.1.call-update) | async-done | bytes 2097168 | tf_op jit(solution)/shard_map/all_gather | solution.py:160
  215.9 2.3 multiply_reduce_fusion.3
  218.2 5.7 %psum.31 = f32[32]{0:T(128)S(1)} all-reduce(f32[32]{0:T(128)S(1)} %get-tuple-element.34), channel_id=1, replica_groups=mesh['ep'=8,'tp'=4] {'tp'}, use_global_device_ids=true, to_apply=%region_18.19 | all-reduce | flops 32 | bytes 256 | tf_op jit(solution)/shard_map/psum | solution.py:165
  223.9 0.7 add_convert_fusion
  (83 shorter events, 1.2 us)
Async XLA Ops:
  8.0 84.9 %copy-start = (bf16[1,256,2048]{2,1,0:T(8,128)(2,1)S(1)}, bf16[1,256,2048]{2,1,0:T(8,128)(2,1)}, u32[]{:S(2)}) copy-start(bf16[1,256,2048]{2,1,0:T(8,128)(2,1)} %param.48) | copy-start | bytes 3145732
  8.0 7.3 %copy-start.1 = (bf16[32,2048]{1,0:T(8,128)(2,1)S(1)}, bf16[32,2048]{1,0:T(8,128)(2,1)}, u32[]{:S(2)}) copy-start(bf16[32,2048]{1,0:T(8,128)(2,1)} %param.27) | copy-start | bytes 393220
  8.0 6.2 %copy-start.10 = (bf16[3,4,128]{2,1,0:T(4,128)(2,1)S(1)}, bf16[3,4,128]{2,1,0:T(4,128)(2,1)}, u32[]{:S(2)}) copy-start(bf16[3,4,128]{2,1,0:T(4,128)(2,1)} %param.36) | copy-start | bytes 9220
  8.0 8.2 %copy-start.15 = (f32[2]{0:T(128)S(1)}, f32[2]{0:T(128)}, u32[]{:S(2)}) copy-start(f32[2]{0:T(128)} %param.35) | copy-start | bytes 28
  8.0 8.2 %copy-start.12 = (f32[2]{0:T(128)S(1)}, f32[2]{0:T(128)}, u32[]{:S(2)}) copy-start(f32[2]{0:T(128)} %param.34) | copy-start | bytes 28
  8.1 8.6 %copy-start.2 = (f32[32,2,64,128]{3,2,1,0:T(8,128)S(1)}, f32[32,2,64,128]{3,2,1,0:T(8,128)}, u32[]{:S(2)}) copy-start(f32[32,2,64,128]{3,2,1,0:T(8,128)} %param.38) | copy-start | bytes 6291460
  8.1 47.9 %all-reduce.4.cloned.1.call-start = ((), (), s32[]{:S(2)}) async-start(), calls=%async_computation.3 | async-start | bytes 262144 | tf_op jit(solution)/shard_map/psum | solution.py:83
  16.7 2.2 copy-start.16
  16.7 4.6 %copy-start.6 = (s32[32,4]{0,1:T(4,128)S(1)}, s32[32,4]{0,1:T(4,128)}, u32[]{:S(2)}) copy-start(s32[32,4]{0,1:T(4,128)} %param.45) | copy-start | bytes 1540
  16.7 5.5 %copy-start.7 = (bf16[2048]{0:T(1024)(128)(2,1)S(1)}, bf16[2048]{0:T(1024)(128)(2,1)}, u32[]{:S(2)}) copy-start(bf16[2048]{0:T(1024)(128)(2,1)} %param.41) | copy-start | bytes 12292
  16.7 5.5 %copy-start.8 = (bf16[2048]{0:T(1024)(128)(2,1)S(1)}, bf16[2048]{0:T(1024)(128)(2,1)}, u32[]{:S(2)}) copy-start(bf16[2048]{0:T(1024)(128)(2,1)} %param.42) | copy-start | bytes 12292
  21.3 136.0 %reduce-scatter.2.cloned.1.call-start = ((), (), s32[]{:S(2)}) async-start(), calls=%async_computation.4 | async-start | bytes 1310720 | tf_op jit(solution)/shard_map/reduce_scatter | solution.py:122
  58.6 33.3 %copy-start.3 = (bf16[1,2048,256]{2,1,0:T(8,128)(2,1)S(1)}, bf16[1,2048,256]{2,1,0:T(8,128)(2,1)}, u32[]{:S(2)}) copy-start(bf16[1,2048,256]{2,1,0:T(8,128)(2,1)} %param.46) | copy-start | bytes 3145732
  61.7 30.6 %copy-start.13 = (bf16[1,2048,256]{2,1,0:T(8,128)(2,1)S(1)}, bf16[1,2048,256]{2,1,0:T(8,128)(2,1)}, u32[]{:S(2)}) copy-start(bf16[1,2048,256]{2,1,0:T(8,128)(2,1)} %param.47) | copy-start | bytes 3145732
  92.8 2.1 copy-start.4
  92.8 19.1 %copy-start.9 = (bf16[2048]{0:T(1024)(128)(2,1)S(1)}, bf16[2048]{0:T(1024)(128)(2,1)}, u32[]{:S(2)}) copy-start(bf16[2048]{0:T(1024)(128)(2,1)} %param.49) | copy-start | bytes 12292
  92.8 19.1 %copy-start.11 = (bf16[512]{0:T(512)(128)(2,1)S(1)}, bf16[512]{0:T(512)(128)(2,1)}, u32[]{:S(2)}) copy-start(bf16[512]{0:T(512)(128)(2,1)} %param.53) | copy-start | bytes 3076
  92.8 19.8 %copy-start.5 = (bf16[2048,8]{0,1:T(8,128)(2,1)S(1)}, bf16[2048,8]{0,1:T(8,128)(2,1)}, u32[]{:S(2)}) copy-start(bf16[2048,8]{0,1:T(8,128)(2,1)} %param.44) | copy-start | bytes 98308
  92.8 30.0 %copy-start.14 = (bf16[2048,2]{0,1:T(2,128)(2,1)S(1)}, bf16[2048,2]{0,1:T(2,128)(2,1)}, u32[]{:S(2)}) copy-start(bf16[2048,2]{0,1:T(2,128)(2,1)} %param.43) | copy-start | bytes 24580
  94.3 71.2 %all-gather.3.cloned.1.call-start = ((), (), s32[]{:S(2)}) async-start(), calls=%async_computation.5 | async-start | bytes 2359296 | tf_op jit(solution)/shard_map/all_gather | solution.py:148
  94.9 121.0 %all-gather.5.cloned.1.call-start = ((), (), s32[]{:S(2)}) async-start(), calls=%async_computation.6 | async-start | bytes 2359296 | tf_op jit(solution)/shard_map/all_gather | solution.py:160
  95.0 14.5 %collective-permute-start = (bf16[256,512]{1,0:T(8,128)(2,1)S(1)}, bf16[256,512]{1,0:T(8,128)(2,1)S(1)}, u32[]{:S(2)}, u32[]{:S(2)}) collective-permute-start(bf16[256,512]{1,0:T(8,128)(2,1)S(1)} %copy-done.4), channel_id=1, source_target_pairs={{0,4},{4,8},{8,12},{12,16},{16,20},{20,24},{24,28},{28,0},{1,5},{5... | collective-permute-start | bytes 786440 | tf_op jit(solution)/shard_map/ppermute | solution.py:141
  96.4 26.6 %collective-permute-start.4 = (bf16[256,512]{1,0:T(8,128)(2,1)S(1)}, bf16[256,512]{1,0:T(8,128)(2,1)S(1)}, u32[]{:S(2)}, u32[]{:S(2)}) collective-permute-start(bf16[256,512]{1,0:T(8,128)(2,1)S(1)} %copy-done.4), channel_id=1, source_target_pairs={{0,28},{4,0},{8,4},{12,8},{16,12},{20,16},{24,20},{28,24},{1,29},{... | collective-permute-start | bytes 786440 | tf_op jit(solution)/shard_map/ppermute | solution.py:142
  109.4 13.4 %collective-permute-start.1 = (bf16[256,512]{1,0:T(8,128)(2,1)S(1)}, bf16[256,512]{1,0:T(8,128)(2,1)S(1)}, u32[]{:S(2)}, u32[]{:S(2)}) collective-permute-start(bf16[256,512]{1,0:T(8,128)(2,1)S(1)} %collective-permute-done), channel_id=1, source_target_pairs={{0,4},{4,8},{8,12},{12,16},{16,20},{20,24},{24,28},{28,0},{1,5},{5... | collective-permute-start | bytes 786440 | tf_op jit(solution)/shard_map/ppermute | solution.py:141
  122.8 15.0 %collective-permute-start.2 = (bf16[256,512]{1,0:T(8,128)(2,1)S(1)}, bf16[256,512]{1,0:T(8,128)(2,1)S(1)}, u32[]{:S(2)}, u32[]{:S(2)}) collective-permute-start(bf16[256,512]{1,0:T(8,128)(2,1)S(1)} %collective-permute-done.1), channel_id=1, source_target_pairs={{0,4},{4,8},{8,12},{12,16},{16,20},{20,24},{24,28},{28,0},{1,5},{5... | collective-permute-start | bytes 786440 | tf_op jit(solution)/shard_map/ppermute | solution.py:141
  123.1 19.5 %collective-permute-start.5 = (bf16[256,512]{1,0:T(8,128)(2,1)S(1)}, bf16[256,512]{1,0:T(8,128)(2,1)S(1)}, u32[]{:S(2)}, u32[]{:S(2)}) collective-permute-start(bf16[256,512]{1,0:T(8,128)(2,1)S(1)} %collective-permute-done.4), channel_id=1, source_target_pairs={{0,28},{4,0},{8,4},{12,8},{16,12},{20,16},{24,20},{28,24},{1,29},{... | collective-permute-start | bytes 786440 | tf_op jit(solution)/shard_map/ppermute | solution.py:142
  137.9 14.8 %collective-permute-start.3 = (bf16[256,512]{1,0:T(8,128)(2,1)S(1)}, bf16[256,512]{1,0:T(8,128)(2,1)S(1)}, u32[]{:S(2)}, u32[]{:S(2)}) collective-permute-start(bf16[256,512]{1,0:T(8,128)(2,1)S(1)} %collective-permute-done.2), channel_id=1, source_target_pairs={{0,4},{4,8},{8,12},{12,16},{16,20},{20,24},{24,28},{28,0},{1,5},{5... | collective-permute-start | bytes 786440 | tf_op jit(solution)/shard_map/ppermute | solution.py:141
  142.5 13.8 %collective-permute-start.6 = (bf16[256,512]{1,0:T(8,128)(2,1)S(1)}, bf16[256,512]{1,0:T(8,128)(2,1)S(1)}, u32[]{:S(2)}, u32[]{:S(2)}) collective-permute-start(bf16[256,512]{1,0:T(8,128)(2,1)S(1)} %collective-permute-done.5), channel_id=1, source_target_pairs={{0,28},{4,0},{8,4},{12,8},{16,12},{20,16},{24,20},{28,24},{1,29},{... | collective-permute-start | bytes 786440 | tf_op jit(solution)/shard_map/ppermute | solution.py:142
  157.3 11.6 %all-to-all-start.1 = ((bf16[8,32,512]{2,1,0:T(8,128)(2,1)}), bf16[8,32,512]{2,1,0:T(8,128)(2,1)S(1)}, u32[]{:S(2)}, u32[]{:S(2)}) async-start(bf16[8,32,512]{2,1,0:T(8,128)(2,1)} %reduce-scatter.2.cloned.1.call-done), calls=%async_computation.2 | async-start | bytes 524288 | tf_op jit(solution)/shard_map/all_to_all | solution.py:123
  160.7 55.2 %all-reduce.6.cloned.1.call-start = ((), (), s32[]{:S(2)}) async-start(), calls=%async_computation.7 | async-start | bytes 524288 | tf_op jit(solution)/shard_map/psum | solution.py:155
Sparse Core Ops, SparseCore 0:
  21.4 34.5 all-reduce.3
  94.4 23.0 reduce-scatter.1
  168.6 31.7 all-reduce.5
Sparse Core Ops, SparseCore 1:
  96.9 68.6 all-gather.2
  167.5 48.3 all-gather.4
